TPU v7x, 32 devices: a whole 2x2x4 slice. The times are simulated.
32 devices in a mesh: sp: 8 (over z, core), tp: 4 (over y, x).
Axes of the slice: x: 2, y: 2, z: 4, core: 2. Of those that a mesh axis runs over, the one named last changes fastest.
Arguments:
- moe_input: bfloat16 [1408, 2048], P('sp'), may hold values from -6 to 6
- cotangent: bfloat16 [1408, 2048], P('sp'), may hold values from -6 to 6
- route_ids: int32 [1408, 2], P('sp'), may hold values from 0 to 7, all different within a row; in each aligned block of 176 rows (0 to 175, 176 to 351, ...) at most 88 rows name the same one
- route_weights: float32 [1408, 2], P('sp'), may hold values from 0.25 to 1.5
- expert_gate: bfloat16 [8, 2048, 1024], P('sp', None, 'tp'), may hold values from -0.125 to 0.125
- expert_up: bfloat16 [8, 2048, 1024], P('sp', None, 'tp'), may hold values from -0.125 to 0.125
- expert_down: bfloat16 [8, 1024, 2048], P('sp', 'tp'), may hold values from -0.1875 to 0.1875
- out_proj: bfloat16 [2048, 2048], P('tp'), may hold values from -0.125 to 0.125
- gate_b: bfloat16 [1408, 2048], P('sp', 'tp'), may hold values from -6 to 6
- gate_c: bfloat16 [1408, 2048], P('sp', 'tp'), may hold values from -6 to 6
- conv_in: bfloat16 [1408, 2048], P('sp', 'tp'), may hold values from -6 to 6
- taps: float32 [3, 2048], P(None, 'tp'), may hold values from -4 to 4
Outputs:
- grad_expert_gate: float32 [8, 2048, 1024], P('sp', None, 'tp')
- grad_expert_up: float32 [8, 2048, 1024], P('sp', None, 'tp')
- grad_expert_down: float32 [8, 1024, 2048], P('sp', 'tp')
- grad_out_proj: float32 [2048, 2048], P('tp', 'sp')
- grad_gate_b: bfloat16 [1408, 2048], P('sp', 'tp')
- grad_gate_c: bfloat16 [1408, 2048], P('sp', 'tp')
- grad_conv_in: bfloat16 [1408, 2048], P('sp', 'tp')
Inputs may be any that keep to these rules, and one draw needn't show every extreme that they name: `route_ids`: in the 176 rows of each index of sp, each row names 2 different experts, no expert is named by more than 88 rows, a bound that some block reaches.
All inputs are finite; a program needn't handle non-finite values.
Results may differ from a plain program's by a relative error of at most 0.033.
Values may be sent and summed in bfloat16 or wider, within the bound.
A program may use at most 64 MiB of HBM per device.

v0:
```python
import jax
import jax.numpy as jnp
from jax import lax
from jax.sharding import PartitionSpec as P

EXP_DEV = 1


def passed_along(block, axis, distance):
    devices = range(lax.axis_size(axis))
    route = [(i - distance, i) for i in devices if i - distance in devices]
    return lax.ppermute(block, axis, route)


def slot_table(routes, experts, capacity):
    flattened = routes.reshape(-1)
    onehot = (flattened[:, None] == jnp.arange(experts, dtype=jnp.int32)[None, :]).astype(jnp.int32)
    earlier = jnp.cumsum(onehot, axis=0) - onehot
    return flattened * capacity + jnp.sum(earlier * onehot, axis=1)


def contract(left, right, left_dim, right_dim):
    return lax.dot_general(
        left, right, (((left_dim,), (right_dim,)), ((), ())), preferred_element_type=jnp.float32
    )


def on_device(
    moe_input,
    cotangent,
    route_ids,
    route_weights,
    expert_gate,
    expert_up,
    expert_down,
    out_proj,
    gate_b,
    gate_c,
    conv_in,
    taps,
):
    groups = lax.axis_size("sp")
    lanes = lax.axis_size("tp")
    token_count, model_width = moe_input.shape
    choices_count = route_ids.shape[1]
    experts = EXP_DEV * groups
    capacity = 2 * token_count * choices_count // experts
    assigned = token_count * choices_count
    slice_width = model_width // lanes
    column_start = lax.axis_index("tp") * slice_width
    slots = slot_table(route_ids, experts, capacity)
    owner = (
        jnp.full((experts * capacity,), assigned, jnp.int32)
        .at[slots]
        .set(jnp.arange(assigned, dtype=jnp.int32))
    )
    token_owner = jnp.where(owner < assigned, owner // choices_count, token_count)
    scaled = (
        (route_weights[:, :, None] * cotangent[:, None, :].astype(jnp.float32))
        .astype(jnp.bfloat16)
        .reshape(assigned, model_width)
    )

    def to_slots(values, positions):
        padded = jnp.concatenate([values, jnp.zeros((1, values.shape[1]), values.dtype)], axis=0)
        return padded[positions].reshape(experts, capacity, values.shape[1])

    slim_x = to_slots(
        lax.dynamic_slice_in_dim(moe_input, column_start, slice_width, 1), token_owner
    )
    slim_s = to_slots(lax.dynamic_slice_in_dim(scaled, column_start, slice_width, 1), owner)
    part_x, part_s = (
        lax.all_to_all(slim_x, "sp", split_axis=0, concat_axis=0, tiled=True),
        lax.all_to_all(slim_s, "sp", split_axis=0, concat_axis=0, tiled=True),
    )
    arrived_x, arrived_s = (
        lax.all_gather(part_x, "tp", axis=2, tiled=True),
        lax.all_gather(part_s, "tp", axis=2, tiled=True),
    )
    rows_x = arrived_x.reshape(-1, model_width)
    rows_s = arrived_s.reshape(-1, model_width)
    weight_gate = expert_gate[0]
    weight_up = expert_up[0]
    weight_down = expert_down[0]
    pre_gate = jnp.dot(rows_x, weight_gate, preferred_element_type=jnp.float32)
    pre_up = jnp.dot(rows_x, weight_up, preferred_element_type=jnp.float32)
    sigma = jax.nn.sigmoid(pre_gate)
    active = pre_gate * sigma
    hidden = (active * pre_up).astype(jnp.bfloat16)
    back = contract(rows_s, weight_down, 1, 1)
    grad_pre_gate = (back * pre_up * sigma * (1.0 + pre_gate * (1.0 - sigma))).astype(jnp.bfloat16)
    grad_pre_up = (back * active).astype(jnp.bfloat16)
    grad_down = contract(hidden, rows_s, 0, 0)
    grad_gate = contract(rows_x, grad_pre_gate, 0, 0)
    grad_up = contract(rows_x, grad_pre_up, 0, 0)
    partial_value = contract(grad_pre_gate, weight_gate, 1, 1) + contract(
        grad_pre_up, weight_up, 1, 1
    )
    summed = lax.psum_scatter(
        partial_value.astype(jnp.bfloat16), "tp", scatter_dimension=1, tiled=True
    )
    returned = lax.all_to_all(
        summed.reshape(groups, capacity, slice_width), "sp", split_axis=0, concat_axis=0, tiled=True
    )
    returned = returned.reshape(experts * capacity, slice_width)
    moe_rows = (
        returned[slots]
        .astype(jnp.float32)
        .reshape(token_count, choices_count, slice_width)
        .sum(axis=1)
    )
    own_cols = lax.dynamic_slice_in_dim(cotangent, column_start, slice_width, 1)
    grad_cols = (own_cols.astype(jnp.float32) + moe_rows).astype(jnp.bfloat16)
    stream_grad = lax.all_gather(grad_cols, "tp", axis=1, tiled=True)
    mixed = gate_c.astype(jnp.float32) * conv_in.astype(jnp.float32)
    earlier_rows = passed_along(mixed[-2:], "sp", 1)
    extended = jnp.concatenate([earlier_rows, mixed], axis=0)
    conv = taps[2] * mixed + taps[1] * extended[1:-1] + taps[0] * extended[:-2]
    merged = (gate_b.astype(jnp.float32) * conv).astype(jnp.bfloat16)
    grad_merged = contract(stream_grad, out_proj, 1, 1)
    grad_gate_b = (grad_merged * conv).astype(jnp.bfloat16)
    grad_conv = grad_merged * gate_b.astype(jnp.float32)
    later_rows = passed_along(grad_conv[:2], "sp", -1)
    extended_grad = jnp.concatenate([grad_conv, later_rows], axis=0)
    grad_mixed = taps[2] * grad_conv + taps[1] * extended_grad[1:-1] + taps[0] * extended_grad[2:]
    grad_gate_c = (grad_mixed * conv_in.astype(jnp.float32)).astype(jnp.bfloat16)
    grad_conv_in = (grad_mixed * gate_c.astype(jnp.float32)).astype(jnp.bfloat16)
    grad_proj = lax.psum_scatter(
        contract(stream_grad, merged, 0, 0).astype(jnp.bfloat16),
        "sp",
        scatter_dimension=0,
        tiled=True,
    ).astype(jnp.float32)
    return (
        grad_gate[None],
        grad_up[None],
        grad_down[None],
        grad_proj.T,
        grad_gate_b,
        grad_gate_c,
        grad_conv_in,
    )


def solution(mesh):
    placed = (
        P("sp", None),
        P("sp", None),
        P("sp", None),
        P("sp", None),
        P("sp", None, "tp"),
        P("sp", None, "tp"),
        P("sp", "tp", None),
        P("tp", None),
        P("sp", "tp"),
        P("sp", "tp"),
        P("sp", "tp"),
        P(None, "tp"),
    )
    return jax.shard_map(
        on_device,
        mesh=mesh,
        in_specs=placed,
        out_specs=(
            P("sp", None, "tp"),
            P("sp", None, "tp"),
            P("sp", "tp", None),
            P("tp", "sp"),
            P("sp", "tp"),
            P("sp", "tp"),
            P("sp", "tp"),
        ),
        check_vma=False,
    )
```

profile of v0, /device:TPU:0, one launch (start us, length us, event | category | flops | bytes accessed | tf_op | source)
XLA Modules:
  0.0 263.6 jit_solution(15167065156575614843)
XLA Ops:
  7.2 0.8 broadcast_multiply_fusion
  8.1 0.8 copy.21
  8.9 0.1 copy.20
  9.0 0.1 mul.130
  9.1 0.1 eq.22
  9.3 0.9 reduce-window.6
  10.2 0.2 slice_reduce_fusion
  10.4 0.1 add_bitcast_fusion
  10.6 2.9 %scatter_custom_fusion = s32[704]{0:T(1024)S(1)} fusion(s32[352]{0:T(512)S(1)} %fusion.33, s32[352]{0:T(512)S(1)} %iota.8, s32[]{:T(128)} %constant.14.clone.1), kind=kCustom, calls=%fused_computation.74 | custom fusion | bytes 2820 | tf_op jit(solution)/shard_map/scatter | solution.py:55
  13.5 0.9 constant_dynamic-slice_fusion
  14.5 2.8 %gather_fusion = bf16[704,512]{1,0:T(8,128)(2,1)S(1)} fusion(bf16[177,512]{1,0:T(8,128)(2,1)S(1)} %concatenate.12, s32[1024]{0:T(1024)S(1)} %get-tuple-element.34), kind=kCustom, calls=%fused_computation | custom fusion | bytes 1444608 | tf_op jit(solution)/shard_map/gather | solution.py:66
  17.3 25.8 %all_to_all.15 = bf16[8,88,512]{2,1,0:T(8,128)(2,1)} all-to-all(bf16[8,88,512]{2,1,0:T(8,128)(2,1)S(1)} %bitcast.53), channel_id=1, replica_groups=mesh['sp'=8,'tp'=4] {'sp'}, dimensions={0} | all-to-all | bytes 1441792 | tf_op jit(solution)/shard_map/all_to_all | solution.py:73
  43.2 4.2 %mul.134 = f32[176,2,2048]{2,1,0:T(2,128)} broadcast(bf16[176,2048]{1,0:T(8,128)(2,1)} %param.13), dimensions={0,2} | broadcast | bytes 3604480 | tf_op jit(solution)/shard_map/mul | solution.py:59
  47.4 5.0 %mul.135 = f32[352,2048]{1,0:T(8,128)} reshape(f32[176,2,2048]{2,1,0:T(2,128)} %mul.134) | data formatting | bytes 5767168 | tf_op jit(solution)/shard_map/mul | solution.py:59
  52.4 0.1 copy.22
  52.5 0.1 mul.132
  52.7 1.2 fusion.9
  54.0 2.8 %gather_fusion.1 = bf16[704,512]{1,0:T(8,128)(2,1)S(1)} fusion(bf16[353,512]{1,0:T(8,128)(2,1)S(1)} %concatenate.13, s32[1024]{0:T(1024)S(1)} %get-tuple-element.33), kind=kCustom, calls=%fused_computation.1 | custom fusion | bytes 1444608 | tf_op jit(solution)/shard_map/gather | solution.py:66
  56.8 22.6 %all_to_all.16 = bf16[8,88,512]{2,1,0:T(8,128)(2,1)} all-to-all(bf16[8,88,512]{2,1,0:T(8,128)(2,1)S(1)} %bitcast.54), channel_id=1, replica_groups=mesh['sp'=8,'tp'=4] {'sp'}, dimensions={0} | all-to-all | bytes 1441792 | tf_op jit(solution)/shard_map/all_to_all | solution.py:74
  79.5 4.3 %all-gather.3.cloned.1.call-done = bf16[8,88,2048]{2,1,0:T(8,128)(2,1)} async-done(((bf16[8,88,512]{2,1,0:T(8,128)(2,1)}), bf16[8,88,2048]{2,1,0:T(8,128)(2,1)}) %all-gather.3.cloned.1.call-update) | async-done | bytes 2883600 | tf_op jit(solution)/shard_map/all_gather | solution.py:77
  83.8 4.0 %fusion.2 = f32[704,256]{1,0:T(8,128)} fusion(bf16[704,2048]{1,0:T(8,128)(2,1)} %bitcast.63, bf16[1,2048,256]{2,1,0:T(8,128)(2,1)} %param.16), kind=kOutput, calls=%fused_computation.11 | convolution fusion | flops 738197504 | bytes 4653056 | tf_op jit(solution)/shard_map/dot_general | solution.py:85
  87.8 1.8 fusion.5
  89.6 37.6 %all-gather.5.cloned.1.call-done = bf16[8,88,2048]{2,1,0:T(8,128)(2,1)} async-done(((bf16[8,88,512]{2,1,0:T(8,128)(2,1)}), bf16[8,88,2048]{2,1,0:T(8,128)(2,1)}) %all-gather.5.cloned.1.call-update) | async-done | bytes 2883600 | tf_op jit(solution)/shard_map/all_gather | solution.py:78
  127.2 3.7 %multiply_convert_fusion.1 = (bf16[704,256]{1,0:T(8,128)(2,1)S(1)}, bf16[704,256]{1,0:T(8,128)(2,1)S(1)}) fusion(f32[704,256]{1,0:T(8,128)} %fusion.2, f32[704,256]{1,0:T(8,128)} %fusion.5, bf16[704,2048]{1,0:T(8,128)(2,1)} %bitcast.67, bf16[1,256,2048]{2,1,0:T(8,128)(2,1)} %param.18), kind=kOutput, calls=%fused_computation.21 | convolution fusion | flops 740540416 | bytes 6094848 | tf_op jit(solution)/shard_map/dot_general | solution.py:23
  130.9 0.9 fusion
  131.9 2.6 add_convert_fusion
  134.5 41.9 %reduce-scatter.3.cloned.1.call-done = bf16[704,512]{1,0:T(8,128)(2,1)} async-done(((bf16[704,2048]{1,0:T(8,128)(2,1)}), bf16[704,512]{1,0:T(8,128)(2,1)}) %reduce-scatter.3.cloned.1.call-update) | async-done | bytes 720912 | tf_op jit(solution)/shard_map/reduce_scatter | solution.py:99
  176.3 4.6 %all-to-all-start.2 = ((bf16[8,88,512]{2,1,0:T(8,128)(2,1)}), bf16[8,88,512]{2,1,0:T(8,128)(2,1)S(1)}, u32[]{:S(2)}, u32[]{:S(2)}) async-start(bf16[8,88,512]{2,1,0:T(8,128)(2,1)} %bitcast.55), calls=%async_computation.3 | async-start | bytes 1441792 | tf_op jit(solution)/shard_map/all_to_all | solution.py:102
  181.1 0.6 slice.59
  181.7 2.9 %collective-permute-start = (f32[2,512]{1,0:T(2,128)}, f32[2,512]{1,0:T(2,128)}, u32[]{:S(2)}, u32[]{:S(2)}) collective-permute-start(f32[2,512]{1,0:T(2,128)} %slice.59), channel_id=1, source_target_pairs={{0,4},{4,8},{8,12},{12,16},{16,20},{20,24},{24,28},{1,5},{5,9},{9,... | collective-permute-start | bytes 12296 | tf_op jit(solution)/shard_map/ppermute | solution.py:12
  184.6 0.8 fusion.37
  185.4 15.1 %all-to-all-done.2 = bf16[8,88,512]{2,1,0:T(8,128)(2,1)S(1)} async-done(((bf16[8,88,512]{2,1,0:T(8,128)(2,1)}), bf16[8,88,512]{2,1,0:T(8,128)(2,1)S(1)}, u32[]{:S(2)}, u32[]{:S(2)}) %all-to-all-start.2) | async-done | bytes 720928 | tf_op jit(solution)/shard_map/all_to_all | solution.py:102
  200.5 2.0 gather_fusion.2
  202.5 0.5 reshape.93
  203.0 0.8 reduce_sum.22
  203.9 1.0 add_convert_fusion.1
  204.9 11.0 %all_gather.11 = bf16[176,2048]{1,0:T(8,128)(2,1)S(1)} all-gather(bf16[176,512]{1,0:T(8,128)(2,1)S(1)} %add_convert_fusion.1), channel_id=1, replica_groups=mesh['sp'=8,'tp'=4] {'tp'}, dimensions={1}, use_global_device_ids=true | all-gather | bytes 901120 | tf_op jit(solution)/shard_map/all_gather | solution.py:114
  215.9 2.5 multiply_convert_fusion.4
  218.4 2.1 convolution_convert_fusion
  220.5 4.3 %convolution_bitcast_fusion.2 = f32[1,2048,256]{2,1,0:T(8,128)} fusion(bf16[704,2048]{1,0:T(8,128)(2,1)} %bitcast.64, bf16[704,256]{1,0:T(8,128)(2,1)S(1)} %copy-done.4), kind=kOutput, calls=%fused_computation.8 | convolution fusion | flops 738197504 | bytes 5341184 | tf_op jit(solution)/shard_map/dot_general | solution.py:23
  224.9 2.4 convolution_bitcast_fusion
  227.3 1.4 collective-permute-start.1
  228.7 2.4 convolution_bitcast_fusion.1
  231.1 0.8 fusion.20
  231.9 0.7 fusion.21
  232.6 22.4 %reduce-scatter.5.cloned.1.call-done = bf16[256,512]{1,0:T(8,128)(2,1)} async-done(((bf16[2048,512]{1,0:T(8,128)(2,1)}), bf16[256,512]{1,0:T(8,128)(2,1)}) %reduce-scatter.5.cloned.1.call-update) | async-done | bytes 262160 | tf_op jit(solution)/shard_map/reduce_scatter | solution.py:128
  255.0 1.0 convert_bitcast_fusion
  256.0 1.0 copy.23
  (59 shorter events, 0.5 us)
Async XLA Ops:
  7.2 208.7 %copy-start = (bf16[512,2048]{1,0:T(8,128)(2,1)S(1)}, bf16[512,2048]{1,0:T(8,128)(2,1)}, u32[]{:S(2)}) copy-start(bf16[512,2048]{1,0:T(8,128)(2,1)} %param.19) | copy-start | bytes 6291460
  7.2 76.6 %all-gather.3.cloned.1.call-start = ((), (), s32[]{:S(2)}) async-start(), calls=%async_computation.5 | async-start | bytes 3604480 | tf_op jit(solution)/shard_map/all_gather | solution.py:77
  43.1 84.0 %all-gather.5.cloned.1.call-start = ((), (), s32[]{:S(2)}) async-start(), calls=%async_computation.6 | async-start | bytes 3604480 | tf_op jit(solution)/shard_map/all_gather | solution.py:78
  47.4 5.1 %copy-start.12 = (f32[176,2]{0,1:T(2,128)S(1)}, f32[176,2]{0,1:T(2,128)}, u32[]{:S(2)}) copy-start(f32[176,2]{0,1:T(2,128)} %param.15) | copy-start | bytes 4228
  79.5 8.3 %copy-start.2 = (bf16[1,2048,256]{2,1,0:T(8,128)(2,1)S(1)}, bf16[1,2048,256]{2,1,0:T(8,128)(2,1)}, u32[]{:S(2)}) copy-start(bf16[1,2048,256]{2,1,0:T(8,128)(2,1)} %param.17) | copy-start | bytes 3145732
  79.5 96.9 %reduce-scatter.3.cloned.1.call-start = ((), (), s32[]{:S(2)}) async-start(), calls=%async_computation.7 | async-start | bytes 3604480 | tf_op jit(solution)/shard_map/reduce_scatter | solution.py:99
  83.8 4.0 %copy-start.13 = (bf16[8,88,2048]{2,1,0:T(8,128)(2,1)S(1)}, bf16[8,88,2048]{2,1,0:T(8,128)(2,1)}, u32[]{:S(2)}) copy-start(bf16[8,88,2048]{2,1,0:T(8,128)(2,1)} %all-gather.3.cloned.1.call-done) | copy-start | bytes 8650756
  127.2 3.7 %copy-start.1 = (bf16[1,2048,256]{2,1,0:T(8,128)(2,1)S(1)}, bf16[1,2048,256]{2,1,0:T(8,128)(2,1)}, u32[]{:S(2)}) copy-start(bf16[1,2048,256]{2,1,0:T(8,128)(2,1)} %param.16) | copy-start | bytes 3145732
  130.9 1.0 copy-start.3
  130.9 1.0 copy-start.10
  134.5 46.5 %copy-start.5 = (bf16[176,512]{1,0:T(8,128)(2,1)S(1)}, bf16[176,512]{1,0:T(8,128)(2,1)}, u32[]{:S(2)}) copy-start(bf16[176,512]{1,0:T(8,128)(2,1)} %param.21) | copy-start | bytes 540676
  134.5 46.5 %copy-start.7 = (bf16[176,512]{1,0:T(8,128)(2,1)S(1)}, bf16[176,512]{1,0:T(8,128)(2,1)}, u32[]{:S(2)}) copy-start(bf16[176,512]{1,0:T(8,128)(2,1)} %param.22) | copy-start | bytes 540676
  176.3 24.1 %all-to-all-start.2 = ((bf16[8,88,512]{2,1,0:T(8,128)(2,1)}), bf16[8,88,512]{2,1,0:T(8,128)(2,1)S(1)}, u32[]{:S(2)}, u32[]{:S(2)}) async-start(bf16[8,88,512]{2,1,0:T(8,128)(2,1)} %bitcast.55), calls=%async_computation.3 | async-start | bytes 1441792 | tf_op jit(solution)/shard_map/all_to_all | solution.py:102
  180.9 74.1 %reduce-scatter.5.cloned.1.call-start = ((), (), s32[]{:S(2)}) async-start(), calls=%async_computation.8 | async-start | bytes 2359296 | tf_op jit(solution)/shard_map/reduce_scatter | solution.py:128
  181.7 34.2 %collective-permute-start = (f32[2,512]{1,0:T(2,128)}, f32[2,512]{1,0:T(2,128)}, u32[]{:S(2)}, u32[]{:S(2)}) collective-permute-start(f32[2,512]{1,0:T(2,128)} %slice.59), channel_id=1, source_target_pairs={{0,4},{4,8},{8,12},{12,16},{16,20},{20,24},{24,28},{1,5},{5,9},{9,... | collective-permute-start | bytes 12296 | tf_op jit(solution)/shard_map/ppermute | solution.py:12
  203.8 14.5 %copy-start.9 = (bf16[176,512]{1,0:T(8,128)(2,1)S(1)}, bf16[176,512]{1,0:T(8,128)(2,1)}, u32[]{:S(2)}) copy-start(bf16[176,512]{1,0:T(8,128)(2,1)} %param.20) | copy-start | bytes 540676
  218.4 2.1 copy-start.4
  220.5 4.4 %copy-start.15 = (bf16[8,88,2048]{2,1,0:T(8,128)(2,1)S(1)}, bf16[8,88,2048]{2,1,0:T(8,128)(2,1)}, u32[]{:S(2)}) copy-start(bf16[8,88,2048]{2,1,0:T(8,128)(2,1)} %all-gather.5.cloned.1.call-done) | copy-start | bytes 8650756
  220.5 4.4 %copy-start.16 = (f32[704,256]{1,0:T(8,128)S(1)}, f32[704,256]{1,0:T(8,128)}, u32[]{:S(2)}) copy-start(f32[704,256]{1,0:T(8,128)} %fusion.2) | copy-start | bytes 2162692
  220.5 4.3 %copy-start.17 = (f32[704,256]{1,0:T(8,128)S(1)}, f32[704,256]{1,0:T(8,128)}, u32[]{:S(2)}) copy-start(f32[704,256]{1,0:T(8,128)} %fusion.5) | copy-start | bytes 2162692
  224.8 3.8 %copy-start.11 = (bf16[704,256]{1,0:T(8,128)(2,1)S(1)}, bf16[704,256]{1,0:T(8,128)(2,1)}, u32[]{:S(2)}) copy-start(bf16[704,256]{1,0:T(8,128)(2,1)} %copy-done.10) | copy-start | bytes 1081348
  224.8 3.8 %copy-start.14 = (bf16[8,88,2048]{2,1,0:T(8,128)(2,1)S(1)}, bf16[8,88,2048]{2,1,0:T(8,128)(2,1)}, u32[]{:S(2)}) copy-start(bf16[8,88,2048]{2,1,0:T(8,128)(2,1)} %all-gather.3.cloned.1.call-done) | copy-start | bytes 8650756
  227.2 3.8 %copy-start.6 = (bf16[176,512]{1,0:T(8,128)(2,1)S(1)}, bf16[176,512]{1,0:T(8,128)(2,1)}, u32[]{:S(2)}) copy-start(bf16[176,512]{1,0:T(8,128)(2,1)} %param.21) | copy-start | bytes 540676
  227.2 4.7 %copy-start.8 = (bf16[176,512]{1,0:T(8,128)(2,1)S(1)}, bf16[176,512]{1,0:T(8,128)(2,1)}, u32[]{:S(2)}) copy-start(bf16[176,512]{1,0:T(8,128)(2,1)} %param.22) | copy-start | bytes 540676
  227.3 3.8 %collective-permute-start.1 = (f32[2,512]{1,0:T(2,128)S(1)}, f32[2,512]{1,0:T(2,128)S(1)}, u32[]{:S(2)}, u32[]{:S(2)}) collective-permute-start(f32[2,512]{1,0:T(2,128)S(1)} %slice.62), channel_id=1, source_target_pairs={{4,0},{8,4},{12,8},{16,12},{20,16},{24,20},{28,24},{5,1},{9,5},{13... | collective-permute-start | bytes 12296 | tf_op jit(solution)/shard_map/ppermute | solution.py:12
Sparse Core Ops, SparseCore 0:
  43.3 40.4 all-gather.2
  85.6 41.5 all-gather.4
  134.6 41.6 reduce-scatter.2
  220.6 34.3 reduce-scatter.4
where the time goes:
time: 264 us
  waiting for transfers between devices  121 us (46%)
  blocking collectives  59.4 us (22%)
  matrix products  26.7 us (10%)
  local copies, waits for them, and re-layouts  25.4 us (10%)
  between operations  14.1 us (5%)
  starting transfers between devices  9.11 us (3%)
  other arithmetic  7.55 us (3%)
    reduce_scatter x1, waiting for transfers between devices, on_device(): lax.psum_scatter(partial_value.astype(jnp.bfloat16), 'tp', scatter_dimens...  41.9 us
    all_gather x1, waiting for transfers between devices, on_device(): lax.all_gather(part_s, 'tp', axis=2, tiled=True)  37.6 us
    all_to_all x1, blocking collectives, on_device(): lax.all_to_all(slim_x, 'sp', split_axis=0, concat_axis=0, tiled=True)  25.8 us
    all_to_all x1, blocking collectives, on_device(): lax.all_to_all(slim_s, 'sp', split_axis=0, concat_axis=0, tiled=True)  22.6 us
    reduce_scatter x1, waiting for transfers between devices, on_device(): lax.psum_scatter(contract(stream_grad, merged, 0, 0).astype(jnp.bfloat16)...  22.4 us
    dot_general x8, matrix products, contract(): lax.dot_general(left, right, (((left_dim,), (right_dim,)), ((), ())), pre...  20.9 us
    all_to_all x1, waiting for transfers between devices, on_device(): lax.all_to_all(summed.reshape(groups, capacity, slice_width), 'sp', split...  15.1 us
    all_gather x1, blocking collectives, on_device(): stream_grad = lax.all_gather(grad_cols, 'tp', axis=1, tiled=True)  11 us
  transfers between devices with their start and end apart: 7, of which 5 were waited for; matrix products, arithmetic and copies ran while one was open for 14% of the time, Pallas kernels for 0%

commit v1 on v0

--- a/solution.py
+++ b/solution.py
@@ -1,6 +1,9 @@
+import functools
 import jax
 import jax.numpy as jnp
 from jax import lax
+from jax.experimental import pallas as pl
+from jax.experimental.pallas import tpu as pltpu
 from jax.sharding import PartitionSpec as P
 
 EXP_DEV = 1
@@ -25,7 +28,7 @@
     )
 
 
-def on_device(
+def slot_plan(
     moe_input,
     cotangent,
     route_ids,
@@ -142,6 +145,423 @@
     )
 
 
+MESH = pl.DeviceIdType.MESH
+
+
+def place():
+    sp, t = lax.axis_index("sp"), lax.axis_index("tp")
+    return sp, lax.div(sp, 2), lax.rem(sp, 2), t
+
+
+def flipped(t, bits):
+    x, y = lax.rem(t, 2), lax.div(t, 2)
+    if bits & 1:
+        x = 1 - x
+    if bits & 2:
+        y = 1 - y
+    return 2 * y + x
+
+
+def greet(devices):
+    barrier = pltpu.get_barrier_semaphore()
+    for device, exists in devices:
+        @pl.when(exists)
+        def _():
+            pl.semaphore_signal(barrier, inc=1, device_id=device, device_id_type=MESH)
+    pl.semaphore_wait(barrier, sum([jnp.where(exists, 1, 0) for _, exists in devices]))
+
+
+def gather_kernel(
+    stacks, x_ref, s_ref, m_ref, full_x, full_s, full_m,
+    zs, zr, xs, xr, ys, yr, ax, ar, bx, br, cs, cr, own_s, own_r, local,
+):
+    sp, z, c, t = place()
+    rows, width = x_ref.shape
+    quarter = width // 4
+    half = quarter // 2
+    partner = (2 * z + 1 - c, t)
+    up, down = (sp + 2, t), (sp - 2, t)
+    tx, ty, td = flipped(t, 1), flipped(t, 2), flipped(t, 3)
+    always = z >= 0
+    greet([
+        (partner, always), ((sp, tx), always), ((sp, ty), always),
+        (up, z < stacks - 1), (down, z > 0),
+    ])
+    ins, outs = (x_ref, s_ref, m_ref), (full_x, full_s, full_m)
+
+    def cols(q, part=None):
+        if part is None:
+            return pl.ds(pl.multiple_of(q * quarter, 128), quarter)
+        return pl.ds(pl.multiple_of(q * quarter + part * half, 128), half)
+
+    def span(d):
+        return pl.ds(pl.multiple_of((2 * d + c) * rows, 16), rows)
+
+    def remote(src, dst, send, recv, device):
+        return pltpu.make_async_remote_copy(
+            src_ref=src, dst_ref=dst, send_sem=send, recv_sem=recv,
+            device_id=device, device_id_type=MESH,
+        )
+
+    def region(a, d, q, part=None):
+        if a == 2:
+            return outs[2].at[span(d), :]
+        return outs[a].at[span(d), cols(q, part)]
+
+    def mine(a):
+        return m_ref if a == 2 else ins[a].at[:, cols(t)]
+
+    def slot(a, way, k):
+        return (a * 2 + way) * (stacks - 1) + k
+
+    def zcopy(a, way, k, src, d):
+        i = slot(a, way, k)
+        return remote(src, region(a, d, t), zs.at[i], zr.at[i], up if way == 0 else down)
+
+    def ahead(way):
+        return z < stacks - 1 if way == 0 else z > 0
+
+    def source(way, k):
+        return z - 1 - k if way == 0 else z + 1 + k
+
+    def exists(way, k):
+        return z >= k + 1 if way == 0 else z + 1 + k < stacks
+
+    order = (0, 1, 2)
+    for a in order:
+        for way in (0, 1):
+            @pl.when(ahead(way))
+            def _():
+                zcopy(a, way, 0, mine(a), z).start()
+    keeps = []
+    for a in order:
+        dst = outs[a].at[span(z), :]
+        keeps.append(pltpu.make_async_copy(ins[a], dst, local.at[a]))
+        keeps[-1].start()
+        keeps.append(remote(ins[a], dst, own_s.at[a], own_r.at[a], partner))
+        keeps[-1].start()
+
+    def xy(a, way, k, d, kind):
+        i = slot(a, way, k)
+        if kind == "x":
+            r = region(a, d, t)
+            return remote(r, r, xs.at[i], xr.at[i], (sp, tx))
+        if kind == "y":
+            r = region(a, d, t)
+            return remote(r, r, ys.at[i], yr.at[i], (sp, ty))
+        if kind == "a":
+            r = region(a, d, tx, 0)
+            return remote(r, r, ax.at[i], ar.at[i], (sp, ty))
+        r = region(a, d, ty, 1)
+        return remote(r, r, bx.at[i], br.at[i], (sp, tx))
+
+    def shared(a, way, k, d, which):
+        i = 4 * slot(a, way, k) + which
+        r = region(a, d, (t, tx, ty, td)[which])
+        return remote(r, r, cs.at[i], cr.at[i], partner)
+
+    def first(a, way, k):
+        d = source(way, k)
+        zcopy(a, way, k, region(a, d, t), d).wait_recv()
+        if k < stacks - 2:
+            @pl.when(ahead(way))
+            def _():
+                zcopy(a, way, k + 1, region(a, d, t), d).start()
+        if a < 2:
+            xy(a, way, k, d, "x").start()
+            xy(a, way, k, d, "y").start()
+        shared(a, way, k, d, 0).start()
+
+    def second(a, way, k):
+        d = source(way, k)
+        if a < 2:
+            xy(a, way, k, d, "x").wait_recv()
+            xy(a, way, k, d, "a").start()
+            shared(a, way, k, d, 1).start()
+            xy(a, way, k, d, "y").wait_recv()
+            xy(a, way, k, d, "b").start()
+            shared(a, way, k, d, 2).start()
+
+    def third(a, way, k):
+        d = source(way, k)
+        if a < 2:
+            xy(a, way, k, d, "a").wait_recv()
+            xy(a, way, k, d, "b").wait_recv()
+            shared(a, way, k, d, 3).start()
+
+    steps = [(a, way, k) for k in range(stacks - 1) for a in order for way in (0, 1)]
+    for i in range(len(steps) + 4):
+        for stage, lag in ((first, 0), (second, 2), (third, 4)):
+            if 0 <= i - lag < len(steps):
+                a, way, k = steps[i - lag]
+                @pl.when(exists(way, k))
+                def _():
+                    stage(a, way, k)
+    for copy in keeps:
+        copy.wait()
+    for a, way, k in steps:
+        passed = z >= k if way == 0 else z + k < stacks
+
+        @pl.when(passed & ahead(way))
+        def _():
+            d = z - k if way == 0 else z + k
+            zcopy(a, way, k, region(a, d, t), d).wait_send()
+
+        @pl.when(exists(way, k))
+        def _():
+            d = source(way, k)
+            if a < 2:
+                for kind in "xyab":
+                    xy(a, way, k, d, kind).wait_send()
+            for which in range(4 if a < 2 else 1):
+                shared(a, way, k, d, which).wait()
+
+
+def return_kernel(
+    stacks, p_ref, c_ref, stream, columns,
+    theirs, ours, summed, in_x, in_y, out_a, out_b, got_x, got_y, block, blocks, cols,
+    ps, pr, as_, ar, bs, br, xs, xr, ys, yr, zs, zr, gs, gr, es, er, local, load,
+):
+    sp, z, c, t = place()
+    rows, width = p_ref.shape[0] // (2 * stacks), p_ref.shape[1]
+    quarter = width // 4
+    half = quarter // 2
+    partner = (2 * z + 1 - c, t)
+    tx, ty, td = flipped(t, 1), flipped(t, 2), flipped(t, 3)
+    always = z >= 0
+
+    def other_stack(k):
+        return lax.rem(z + k, stacks)
+
+    others = [(partner, always)] + [((sp, u), always) for u in (tx, ty, td)]
+    for k in range(1, stacks):
+        for core in (c, 1 - c):
+            others.append(((2 * other_stack(k) + core, t), always))
+    greet(others)
+
+    def remote(src, dst, send, recv, device):
+        return pltpu.make_async_remote_copy(
+            src_ref=src, dst_ref=dst, send_sem=send, recv_sem=recv,
+            device_id=device, device_id_type=MESH,
+        )
+
+    def span(d, core):
+        return pl.ds(pl.multiple_of((2 * d + core) * rows, 16), rows)
+
+    def wide(q):
+        return pl.ds(pl.multiple_of(q * quarter, 128), quarter)
+
+    def part(q, p):
+        return pl.ds(pl.multiple_of(q * quarter + p * half, 128), half)
+
+    order = list(range(1, stacks)) + [0]
+
+    def swap(k):
+        return remote(p_ref.at[span(other_stack(k), 1 - c), :], theirs.at[k], ps.at[k], pr.at[k], partner)
+
+    def read(k):
+        return pltpu.make_async_copy(p_ref.at[span(other_stack(k), c), :], ours.at[k], load.at[k])
+
+    def via_x(k):
+        return remote(out_b.at[k], in_x.at[k], bs.at[k], br.at[k], (sp, tx))
+
+    def via_y(k):
+        return remote(out_a.at[k], in_y.at[k], as_.at[k], ar.at[k], (sp, ty))
+
+    def to_x(k):
+        return remote(summed.at[k, 0], got_x.at[k], xs.at[k], xr.at[k], (sp, tx))
+
+    def to_y(k):
+        return remote(summed.at[k, 1], got_y.at[k], ys.at[k], yr.at[k], (sp, ty))
+
+    def home(k):
+        back = stacks - k
+        return remote(block.at[k], blocks.at[k], zs.at[k], zr.at[k], (2 * other_stack(k) + c, t))
+
+    def both(k, at):
+        return ours[k, :, at].astype(jnp.float32) + theirs[k, :, at].astype(jnp.float32)
+
+    def stage_one(k):
+        read(k).wait()
+        swap(k).wait_recv()
+        out_a[k] = both(k, part(td, 0)).astype(jnp.bfloat16)
+        via_y(k).start()
+        out_b[k] = both(k, part(td, 1)).astype(jnp.bfloat16)
+        via_x(k).start()
+
+    def stage_two(k):
+        summed[k, 0, :, half:] = both(k, part(tx, 1)).astype(jnp.bfloat16)
+        summed[k, 1, :, :half] = both(k, part(ty, 0)).astype(jnp.bfloat16)
+        via_y(k).wait_recv()
+        summed[k, 0, :, :half] = (both(k, part(tx, 0)) + in_y[k].astype(jnp.float32)).astype(jnp.bfloat16)
+        to_x(k).start()
+        via_x(k).wait_recv()
+        summed[k, 1, :, half:] = (both(k, part(ty, 1)) + in_x[k].astype(jnp.float32)).astype(jnp.bfloat16)
+        to_y(k).start()
+
+    def stage_three(k):
+        mine = both(k, wide(t))
+        to_x(k).wait_recv()
+        to_y(k).wait_recv()
+        mine = mine + got_x[k].astype(jnp.float32) + got_y[k].astype(jnp.float32)
+        block[k] = mine.astype(jnp.bfloat16)
+        if k:
+            home(k).start()
+
+    for k in order:
+        swap(k).start()
+        read(k).start()
+    for i in range(stacks + 2):
+        for stage, lag in ((stage_one, 0), (stage_two, 1), (stage_three, 2)):
+            if 0 <= i - lag < stacks:
+                stage(order[i - lag])
+    total = c_ref[:, wide(t)].astype(jnp.float32) + block[0].astype(jnp.float32)
+    for k in range(1, stacks):
+        home(k).wait_recv()
+        total = total + blocks[k].astype(jnp.float32)
+    cols[...] = total.astype(jnp.bfloat16)
+
+    gathers = []
+    for i, u in enumerate((td, tx, ty)):
+        gathers.append(remote(cols, stream.at[:, wide(t)], gs.at[i], gr.at[i], (sp, u)))
+        gathers[-1].start()
+    keep = pltpu.make_async_copy(cols, stream.at[:, wide(t)], local.at[0])
+    keep.start()
+    for copy in gathers:
+        copy.wait()
+    keep.wait()
+    share = columns.shape[1]
+
+    def slab(device):
+        return stream.at[:, pl.ds(pl.multiple_of(device * share, 128), share)]
+
+    mine = columns.at[pl.ds(pl.multiple_of(sp * rows, 16), rows), :]
+    sends = []
+    n = 0
+    for k in (2, 1, 3, 0) if stacks == 4 else range(stacks):
+        for core in (c, 1 - c) if k else (1 - c,):
+            device = 2 * other_stack(k) + core
+            sends.append(remote(slab(device), mine, es.at[n], er.at[n], (device, t)))
+            sends[-1].start()
+            n += 1
+    keep = pltpu.make_async_copy(slab(sp), mine, local.at[1])
+    keep.start()
+    for k in order:
+        swap(k).wait_send()
+        via_x(k).wait_send()
+        via_y(k).wait_send()
+        to_x(k).wait_send()
+        to_y(k).wait_send()
+        if k:
+            home(k).wait_send()
+    for copy in sends:
+        copy.wait()
+    keep.wait()
+
+
+def dense_plan(
+    moe_input, cotangent, route_ids, route_weights, expert_gate, expert_up,
+    expert_down, out_proj, gate_b, gate_c, conv_in, taps,
+):
+    groups = lax.axis_size("sp")
+    stacks = groups // 2
+    rows, width = moe_input.shape
+    quarter = width // lax.axis_size("tp")
+    tokens = rows * groups
+    bf16 = jnp.bfloat16
+    any_space = pl.BlockSpec(memory_space=pl.ANY)
+    vmem = pl.BlockSpec(memory_space=pltpu.VMEM)
+    dma = pltpu.SemaphoreType.DMA
+
+    mixed = gate_c.astype(jnp.float32) * conv_in.astype(jnp.float32)
+    earlier_rows = passed_along(mixed[-2:], "sp", 1)
+    extended = jnp.concatenate([earlier_rows, mixed], axis=0)
+    conv = taps[2] * mixed + taps[1] * extended[1:-1] + taps[0] * extended[:-2]
+    merged = (gate_b.astype(jnp.float32) * conv).astype(bf16)
+
+    ids = lax.all_gather(route_ids, "sp", axis=0, tiled=True)
+    weights = lax.all_gather(route_weights, "sp", axis=0, tiled=True)
+    chosen = jnp.sum(jnp.where(ids == lax.axis_index("sp"), weights, 0.0), axis=1, keepdims=True)
+
+    n = 6 * (stacks - 1)
+    rows_x, all_cot, all_merged = pl.pallas_call(
+        functools.partial(gather_kernel, stacks),
+        out_shape=(
+            jax.ShapeDtypeStruct((tokens, width), bf16),
+            jax.ShapeDtypeStruct((tokens, width), bf16),
+            jax.ShapeDtypeStruct((tokens, quarter), bf16),
+        ),
+        in_specs=[vmem] * 3,
+        out_specs=(any_space,) * 3,
+        scratch_shapes=[dma((n,))] * 10 + [dma((4 * n,))] * 2 + [dma((3,))] * 3,
+        compiler_params=pltpu.CompilerParams(collective_id=0, has_side_effects=True),
+    )(moe_input, cotangent, merged)
+
+    rows_s = (chosen * all_cot.astype(jnp.float32)).astype(bf16)
+    weight_gate, weight_up, weight_down = expert_gate[0], expert_up[0], expert_down[0]
+    pre_gate = jnp.dot(rows_x, weight_gate, preferred_element_type=jnp.float32)
+    pre_up = jnp.dot(rows_x, weight_up, preferred_element_type=jnp.float32)
+    sigma = jax.nn.sigmoid(pre_gate)
+    active = pre_gate * sigma
+    hidden = (active * pre_up).astype(bf16)
+    back = contract(rows_s, weight_down, 1, 1)
+    grad_pre_gate = (back * pre_up * sigma * (1.0 + pre_gate * (1.0 - sigma))).astype(bf16)
+    grad_pre_up = (back * active).astype(bf16)
+    partial_value = (
+        contract(grad_pre_gate, weight_gate, 1, 1) + contract(grad_pre_up, weight_up, 1, 1)
+    ).astype(bf16)
+    grad_down = contract(hidden, rows_s, 0, 0)
+    grad_gate = contract(rows_x, grad_pre_gate, 0, 0)
+    grad_up = contract(rows_x, grad_pre_up, 0, 0)
+
+    half = quarter // 2
+    share = width // groups
+    scratch = [
+        pltpu.VMEM((stacks, rows, width), bf16),
+        pltpu.VMEM((stacks, rows, width), bf16),
+        pltpu.VMEM((stacks, 2, rows, quarter), bf16),
+    ]
+    scratch += [pltpu.VMEM((stacks, rows, half), bf16)] * 4
+    scratch += [pltpu.VMEM((stacks, rows, quarter), bf16)] * 4
+    scratch += [pltpu.VMEM((rows, quarter), bf16)]
+    scratch += [dma((stacks,))] * 12 + [dma((3,))] * 2 + [dma((groups - 1,))] * 2
+    scratch += [dma((2,)), dma((stacks,))]
+    stream_grad, stream_cols = pl.pallas_call(
+        functools.partial(return_kernel, stacks),
+        out_shape=(
+            jax.ShapeDtypeStruct((rows, width), bf16),
+            jax.ShapeDtypeStruct((tokens, share), bf16),
+        ),
+        in_specs=[any_space, vmem],
+        out_specs=(any_space, any_space),
+        scratch_shapes=scratch,
+        compiler_params=pltpu.CompilerParams(collective_id=1, has_side_effects=True),
+    )(partial_value, cotangent)
+
+    grad_merged = contract(stream_grad, out_proj, 1, 1)
+    grad_gate_b = (grad_merged * conv).astype(bf16)
+    grad_conv = grad_merged * gate_b.astype(jnp.float32)
+    later_rows = passed_along(grad_conv[:2], "sp", -1)
+    extended_grad = jnp.concatenate([grad_conv, later_rows], axis=0)
+    grad_mixed = taps[2] * grad_conv + taps[1] * extended_grad[1:-1] + taps[0] * extended_grad[2:]
+    grad_gate_c = (grad_mixed * conv_in.astype(jnp.float32)).astype(bf16)
+    grad_conv_in = (grad_mixed * gate_c.astype(jnp.float32)).astype(bf16)
+    grad_proj = contract(all_merged, stream_cols, 0, 0)
+    return (
+        grad_gate[None], grad_up[None], grad_down[None], grad_proj,
+        grad_gate_b, grad_gate_c, grad_conv_in,
+    )
+
+
+def on_device(*args):
+    rows, choices = args[2].shape
+    groups, lanes = lax.axis_size("sp"), lax.axis_size("tp")
+    slots = 2 * rows * choices
+    if lanes == 4 and groups % 2 == 0 and groups > 2 and rows * groups <= 2 * slots:
+        return dense_plan(*args)
+    return slot_plan(*args)
+
+
 def solution(mesh):
     placed = (
         P("sp", None),

time: 264 us -> 182 us (0.69)
  the two profiles are of different devices: /device:TPU:0 before, /device:TPU:19 now
where the time goes in v1:
time: 182 us
  Pallas kernels  116 us (64%)
  matrix products  28.4 us (16%)
  blocking collectives  23 us (13%)
  starting transfers between devices  5.68 us (3%)
  other arithmetic  5.26 us (3%)
    pallas_call x1, Pallas kernels, dense_plan(): pl.pallas_call(functools.partial(return_kernel, stacks), out_shape=(jax.S...  65.2 us
    pallas_call x1, Pallas kernels, dense_plan(): pl.pallas_call(functools.partial(gather_kernel, stacks), out_shape=(jax.S...  50.7 us
    dot_general x8, matrix products, contract(): lax.dot_general(left, right, (((left_dim,), (right_dim,)), ((), ())), pre...  21.9 us
    all_gather x1, blocking collectives, dense_plan(): weights = lax.all_gather(route_weights, 'sp', axis=0, tiled=True)  12.9 us
    all_gather x1, blocking collectives, dense_plan(): ids = lax.all_gather(route_ids, 'sp', axis=0, tiled=True)  10.1 us
    ppermute x2, starting transfers between devices, passed_along(): return lax.ppermute(block, axis, route)  5.68 us
    dot_general x1, matrix products, dense_plan(): pre_gate = jnp.dot(rows_x, weight_gate, preferred_element_type=jnp.float32)  4.75 us
  transfers between devices with their start and end apart: 2, of which 1 were waited for; matrix products, arithmetic and copies ran while one was open for 1% of the time, Pallas kernels for 0%

profile of v1, /device:TPU:19, one launch (start us, length us, event | category | flops | bytes accessed | tf_op | source)
XLA Modules:
  0.0 181.9 jit_solution(13340513145686426410)
XLA Ops:
  0.6 0.0 copy-start
  0.6 1.2 convert_multiply_fusion.1
  1.9 3.8 %collective-permute-start = (f32[2,512]{1,0:T(2,128)S(1)}, f32[2,512]{1,0:T(2,128)S(1)}, u32[]{:S(2)}, u32[]{:S(2)}) collective-permute-start(f32[2,512]{1,0:T(2,128)S(1)} %slice.39), channel_id=1, source_target_pairs={{0,4},{4,8},{8,12},{12,16},{16,20},{20,24},{24,28},{1,5},{5,9},{9,... | collective-permute-start | bytes 12296 | tf_op jit(solution)/shard_map/ppermute | solution.py:15
  5.6 0.8 fusion.28
  6.5 10.1 %all-gather = s32[8,176,2]{1,2,0:T(2,128)S(1)} all-gather(s32[1,176,2]{1,2,0:T(2,128)} %bitcast.44), channel_id=1, replica_groups=mesh['sp'=8,'tp'=4] {'sp'}, dimensions={0}, use_global_device_ids=true | all-gather | bytes 12672 | tf_op jit(solution)/shard_map/all_gather | solution.py:482
  16.6 12.9 %all-gather.1 = f32[8,176,2]{1,2,0:T(2,128)S(1)} all-gather(f32[1,176,2]{1,2,0:T(2,128)} %bitcast.45), channel_id=1, replica_groups=mesh['sp'=8,'tp'=4] {'sp'}, dimensions={0}, use_global_device_ids=true | all-gather | bytes 12672 | tf_op jit(solution)/shard_map/all_gather | solution.py:483
  29.5 0.1 reshape.23
  29.6 0.0 collective-permute-done
  29.6 1.7 fusion.18
  31.4 50.7 %shard_map.171 = (bf16[1408,2048]{1,0:T(8,128)(2,1)}, bf16[1408,2048]{1,0:T(8,128)(2,1)}, bf16[1408,512]{1,0:T(8,128)(2,1)}) custom-call(bf16[176,2048]{1,0:T(8,128)(2,1)} %x_ref.1, bf16[176,2048]{1,0:T(8,128)(2,1)} %c_ref.1, bf16[176,512]{1,0:T(8,128)(2,1)} %get-tuple-element.19.m_ref), custom_call_target="tpu_custom_call" | custom-call | tf_op jit(solution)/shard_map/pallas_call | solution.py:487
  82.1 0.0 copy-start.2
  82.1 0.0 copy-start.6
  82.1 0.0 slice-start
  82.1 4.7 %fusion.4 = f32[1408,256]{1,0:T(8,128)S(1)} fusion(bf16[1408,2048]{1,0:T(8,128)(2,1)} %get-tuple-element.12, bf16[1,2048,256]{2,1,0:T(8,128)(2,1)} %param.16), kind=kOutput, calls=%fused_computation.13 | convolution fusion | flops 1476395008 | bytes 8257536 | tf_op jit(solution)/shard_map/dot_general | solution.py:502
  86.9 0.0 copy-done.2
  86.9 0.2 copy-done.6
  87.0 0.0 slice-start.1
  87.0 1.7 fusion.7
  88.7 0.0 slice-done
  88.7 0.2 slice-done.1
  88.9 3.5 %convolution_bitcast_fusion = f32[1,256,2048]{2,1,0:T(8,128)} fusion(bf16[1408,2048]{1,0:T(8,128)(2,1)S(1)} %bitcast.47, f32[1408]{0:T(1024)S(1)} %reshape.23, f32[1408,256]{1,0:T(8,128)S(1)} %fusion.7, f32[1408,256]{1,0:T(8,128)S(1)} %fusion.4), kind=kOutput, calls=%fused_computation.2 | convolution fusion | flops 1487208448 | bytes 10753536 | tf_op jit(solution)/shard_map/dot_general | solution.py:26
  92.4 0.0 copy-done.8
  92.4 2.5 %multiply_convert_fusion.4 = (bf16[1408,256]{1,0:T(8,128)(2,1)S(1)}, bf16[1408,256]{1,0:T(8,128)(2,1)S(1)}) fusion(f32[1408,256]{1,0:T(8,128)S(1)} %fusion.4, f32[1408,256]{1,0:T(8,128)S(1)} %fusion.7, bf16[1,256,2048]{2,1,0:T(8,128)(2,1)S(1)} %copy-done.8, bf16[1408,2048]{1,0:T(8,128)(2,1)S(1)} %bitcast.47, f32[1408]{0:T(1024)S(1)} %reshape.23), kind=kOutput, calls=%fused_computation.7 | convolution fusion | flops 1489731584 | bytes 11146752 | tf_op jit(solution)/shard_map/dot_general | solution.py:26
  95.0 0.0 copy-start.1
  95.0 3.2 %convolution_bitcast_fusion.2 = f32[1,2048,256]{2,1,0:T(8,128)} fusion(bf16[1408,2048]{1,0:T(8,128)(2,1)S(1)} %copy-done.6, bf16[1408,256]{1,0:T(8,128)(2,1)S(1)} %get-tuple-element.22), kind=kOutput, calls=%fused_computation.4 | convolution fusion | flops 1476395008 | bytes 8585216 | tf_op jit(solution)/shard_map/dot_general | solution.py:26
  98.2 0.0 copy-done.1
  98.2 1.7 fusion.2
  99.9 3.2 %convolution_bitcast_fusion.1 = f32[1,2048,256]{2,1,0:T(8,128)} fusion(bf16[1408,2048]{1,0:T(8,128)(2,1)S(1)} %copy-done.6, bf16[1408,256]{1,0:T(8,128)(2,1)S(1)} %get-tuple-element.21), kind=kOutput, calls=%fused_computation.3 | convolution fusion | flops 1476395008 | bytes 8585216 | tf_op jit(solution)/shard_map/dot_general | solution.py:26
  103.2 4.2 %add_convert_fusion.p_ref = bf16[1408,2048]{1,0:T(8,128)(2,1)} fusion(f32[1408,2048]{1,0:T(8,128)S(1)} %fusion.2, bf16[1408,256]{1,0:T(8,128)(2,1)S(1)} %get-tuple-element.21, bf16[1,2048,256]{2,1,0:T(8,128)(2,1)S(1)} %copy-done.2), kind=kOutput, calls=%fused_computation | convolution fusion | flops 1482162176 | bytes 19070976 | tf_op jit(solution)/shard_map/dot_general | solution.py:26
  107.4 65.2 %shard_map.172 = (bf16[176,2048]{1,0:T(8,128)(2,1)}, bf16[1408,256]{1,0:T(8,128)(2,1)}) custom-call(bf16[1408,2048]{1,0:T(8,128)(2,1)} %add_convert_fusion.p_ref, bf16[176,2048]{1,0:T(8,128)(2,1)} %c_ref.1), custom_call_target="tpu_custom_call" | custom-call | tf_op jit(solution)/shard_map/pallas_call | solution.py:529
  172.6 0.0 copy-start.3
  172.6 0.0 copy-done
  172.6 0.0 copy-start.7
  172.6 0.0 copy-start.9
  172.6 2.1 %fusion.30 = f32[176,512]{1,0:T(8,128)S(1)} fusion(bf16[176,2048]{1,0:T(8,128)(2,1)} %get-tuple-element.16, bf16[512,2048]{1,0:T(8,128)(2,1)S(1)} %copy-done), kind=kOutput, calls=%fused_computation.49 | convolution fusion | flops 369098752 | bytes 3178496 | tf_op jit(solution)/shard_map/dot_general | solution.py:26
  174.7 0.0 copy-done.3
  174.7 0.8 convert_multiply_fusion.3
  175.5 1.9 %collective-permute-start.1 = (f32[2,512]{1,0:T(2,128)S(1)}, f32[2,512]{1,0:T(2,128)S(1)}, u32[]{:S(2)}, u32[]{:S(2)}) collective-permute-start(f32[2,512]{1,0:T(2,128)S(1)} %slice.42), channel_id=1, source_target_pairs={{4,0},{8,4},{12,8},{16,12},{20,16},{24,20},{28,24},{5,1},{9,5},{13... | collective-permute-start | bytes 12296 | tf_op jit(solution)/shard_map/ppermute | solution.py:15
  177.4 0.0 copy-done.7
  177.4 0.0 copy-done.9
  177.4 0.0 copy-start.4
  177.4 0.0 copy-start.5
  177.4 1.4 fusion.29
  178.9 1.5 collective-permute-done.1
  180.4 0.0 copy-done.4
  180.4 0.8 fusion.19
  181.2 0.0 copy-done.5
  181.2 0.7 fusion.20
  (5 shorter events, 0.0 us)
Async XLA Ops:
  0.6 171.9 %copy-start = (bf16[512,2048]{1,0:T(8,128)(2,1)S(1)}, bf16[512,2048]{1,0:T(8,128)(2,1)}, u32[]{:S(2)}) copy-start(bf16[512,2048]{1,0:T(8,128)(2,1)} %param.19) | copy-start | bytes 6291460
  1.9 27.8 %collective-permute-start = (f32[2,512]{1,0:T(2,128)S(1)}, f32[2,512]{1,0:T(2,128)S(1)}, u32[]{:S(2)}, u32[]{:S(2)}) collective-permute-start(f32[2,512]{1,0:T(2,128)S(1)} %slice.39), channel_id=1, source_target_pairs={{0,4},{4,8},{8,12},{12,16},{16,20},{20,24},{24,28},{1,5},{5,9},{9,... | collective-permute-start | bytes 12296 | tf_op jit(solution)/shard_map/ppermute | solution.py:15
  82.1 4.8 %copy-start.2 = (bf16[1,2048,256]{2,1,0:T(8,128)(2,1)S(1)}, bf16[1,2048,256]{2,1,0:T(8,128)(2,1)}, u32[]{:S(2)}) copy-start(bf16[1,2048,256]{2,1,0:T(8,128)(2,1)} %param.17) | copy-start | bytes 3145732
  82.1 4.9 %copy-start.6 = (bf16[1408,2048]{1,0:T(8,128)(2,1)S(1)}, bf16[1408,2048]{1,0:T(8,128)(2,1)}, u32[]{:S(2)}) copy-start(bf16[1408,2048]{1,0:T(8,128)(2,1)} %get-tuple-element.12) | copy-start | bytes 17301508
  82.1 6.6 %slice-start = ((s8[5767168]{0:T(1024)(128)(4,1)}), s8[4194304]{0:T(1024)(128)(4,1)S(1)}, s32[]{:S(2)}) async-start(s8[5767168]{0:T(1024)(128)(4,1)} %bitcast.46), calls=%async_computation | async-start | bytes 8388608
  87.0 1.9 %slice-start.1 = ((s8[5767168]{0:T(1024)(128)(4,1)}), s8[1572864]{0:T(1024)(128)(4,1)S(1)}, s32[]{:S(2)}) async-start(s8[5767168]{0:T(1024)(128)(4,1)} %bitcast.46), calls=%async_computation.1 | async-start | bytes 3145728
  88.9 3.5 %copy-start.8 = (bf16[1,256,2048]{2,1,0:T(8,128)(2,1)S(1)}, bf16[1,256,2048]{2,1,0:T(8,128)(2,1)}, u32[]{:S(2)}) copy-start(bf16[1,256,2048]{2,1,0:T(8,128)(2,1)} %param.18) | copy-start | bytes 3145732
  95.0 3.3 %copy-start.1 = (bf16[1,2048,256]{2,1,0:T(8,128)(2,1)S(1)}, bf16[1,2048,256]{2,1,0:T(8,128)(2,1)}, u32[]{:S(2)}) copy-start(bf16[1,2048,256]{2,1,0:T(8,128)(2,1)} %param.16) | copy-start | bytes 3145732
  172.6 2.2 %copy-start.3 = (bf16[176,512]{1,0:T(8,128)(2,1)S(1)}, bf16[176,512]{1,0:T(8,128)(2,1)}, u32[]{:S(2)}) copy-start(bf16[176,512]{1,0:T(8,128)(2,1)} %param.20) | copy-start | bytes 540676
  172.6 4.8 %copy-start.7 = (bf16[1408,512]{1,0:T(8,128)(2,1)S(1)}, bf16[1408,512]{1,0:T(8,128)(2,1)}, u32[]{:S(2)}) copy-start(bf16[1408,512]{1,0:T(8,128)(2,1)} %get-tuple-element.14) | copy-start | bytes 4325380
  172.6 4.8 %copy-start.9 = (bf16[1408,256]{1,0:T(8,128)(2,1)S(1)}, bf16[1408,256]{1,0:T(8,128)(2,1)}, u32[]{:S(2)}) copy-start(bf16[1408,256]{1,0:T(8,128)(2,1)} %get-tuple-element.15) | copy-start | bytes 2162692
  175.5 4.9 %collective-permute-start.1 = (f32[2,512]{1,0:T(2,128)S(1)}, f32[2,512]{1,0:T(2,128)S(1)}, u32[]{:S(2)}, u32[]{:S(2)}) collective-permute-start(f32[2,512]{1,0:T(2,128)S(1)} %slice.42), channel_id=1, source_target_pairs={{4,0},{8,4},{12,8},{16,12},{20,16},{24,20},{28,24},{5,1},{9,5},{13... | collective-permute-start | bytes 12296 | tf_op jit(solution)/shard_map/ppermute | solution.py:15
  177.4 3.0 %copy-start.4 = (bf16[176,512]{1,0:T(8,128)(2,1)S(1)}, bf16[176,512]{1,0:T(8,128)(2,1)}, u32[]{:S(2)}) copy-start(bf16[176,512]{1,0:T(8,128)(2,1)} %param.21) | copy-start | bytes 540676
  177.4 3.8 %copy-start.5 = (bf16[176,512]{1,0:T(8,128)(2,1)S(1)}, bf16[176,512]{1,0:T(8,128)(2,1)}, u32[]{:S(2)}) copy-start(bf16[176,512]{1,0:T(8,128)(2,1)} %param.22) | copy-start | bytes 540676

commit v2 on v1

--- a/solution.py
+++ b/solution.py
@@ -172,8 +172,8 @@
 
 
 def gather_kernel(
-    stacks, x_ref, s_ref, m_ref, full_x, full_s, full_m,
-    zs, zr, xs, xr, ys, yr, ax, ar, bx, br, cs, cr, own_s, own_r, local,
+    stacks, x_ref, s_ref, w_ref, full_x, full_s, full_w,
+    zs, zr, xs, xr, ys, yr, ax, ar, bx, br, cs, cr, ws, wr, own_s, own_r, local,
 ):
     sp, z, c, t = place()
     rows, width = x_ref.shape
@@ -183,11 +183,9 @@
     up, down = (sp + 2, t), (sp - 2, t)
     tx, ty, td = flipped(t, 1), flipped(t, 2), flipped(t, 3)
     always = z >= 0
-    greet([
-        (partner, always), ((sp, tx), always), ((sp, ty), always),
-        (up, z < stacks - 1), (down, z > 0),
-    ])
-    ins, outs = (x_ref, s_ref, m_ref), (full_x, full_s, full_m)
+    peers = [(lax.rem(sp + k, 2 * stacks), t) for k in range(1, 2 * stacks)]
+    greet([(peer, always) for peer in peers + [(sp, tx), (sp, ty)]])
+    ins, outs = (x_ref, s_ref), (full_x, full_s)
 
     def cols(q, part=None):
         if part is None:
@@ -204,12 +202,10 @@
         )
 
     def region(a, d, q, part=None):
-        if a == 2:
-            return outs[2].at[span(d), :]
         return outs[a].at[span(d), cols(q, part)]
 
     def mine(a):
-        return m_ref if a == 2 else ins[a].at[:, cols(t)]
+        return ins[a].at[:, cols(t)]
 
     def slot(a, way, k):
         return (a * 2 + way) * (stacks - 1) + k
@@ -227,13 +223,18 @@
     def exists(way, k):
         return z >= k + 1 if way == 0 else z + 1 + k < stacks
 
-    order = (0, 1, 2)
+    order = (0, 1)
     for a in order:
         for way in (0, 1):
             @pl.when(ahead(way))
             def _():
                 zcopy(a, way, 0, mine(a), z).start()
     keeps = []
+    for k, peer in enumerate(peers):
+        keeps.append(remote(w_ref, full_w.at[sp], ws.at[k], wr.at[k], peer))
+        keeps[-1].start()
+    keeps.append(pltpu.make_async_copy(w_ref, full_w.at[sp], local.at[2]))
+    keeps[-1].start()
     for a in order:
         dst = outs[a].at[span(z), :]
         keeps.append(pltpu.make_async_copy(ins[a], dst, local.at[a]))
@@ -267,27 +268,24 @@
             @pl.when(ahead(way))
             def _():
                 zcopy(a, way, k + 1, region(a, d, t), d).start()
-        if a < 2:
-            xy(a, way, k, d, "x").start()
-            xy(a, way, k, d, "y").start()
+        xy(a, way, k, d, "x").start()
+        xy(a, way, k, d, "y").start()
         shared(a, way, k, d, 0).start()
 
     def second(a, way, k):
         d = source(way, k)
-        if a < 2:
-            xy(a, way, k, d, "x").wait_recv()
-            xy(a, way, k, d, "a").start()
-            shared(a, way, k, d, 1).start()
-            xy(a, way, k, d, "y").wait_recv()
-            xy(a, way, k, d, "b").start()
-            shared(a, way, k, d, 2).start()
+        xy(a, way, k, d, "x").wait_recv()
+        xy(a, way, k, d, "a").start()
+        shared(a, way, k, d, 1).start()
+        xy(a, way, k, d, "y").wait_recv()
+        xy(a, way, k, d, "b").start()
+        shared(a, way, k, d, 2).start()
 
     def third(a, way, k):
         d = source(way, k)
-        if a < 2:
-            xy(a, way, k, d, "a").wait_recv()
-            xy(a, way, k, d, "b").wait_recv()
-            shared(a, way, k, d, 3).start()
+        xy(a, way, k, d, "a").wait_recv()
+        xy(a, way, k, d, "b").wait_recv()
+        shared(a, way, k, d, 3).start()
 
     steps = [(a, way, k) for k in range(stacks - 1) for a in order for way in (0, 1)]
     for i in range(len(steps) + 4):
@@ -310,17 +308,17 @@
         @pl.when(exists(way, k))
         def _():
             d = source(way, k)
-            if a < 2:
-                for kind in "xyab":
-                    xy(a, way, k, d, kind).wait_send()
-            for which in range(4 if a < 2 else 1):
+            for kind in "xyab":
+                xy(a, way, k, d, kind).wait_send()
+            for which in range(4):
                 shared(a, way, k, d, which).wait()
 
 
 def return_kernel(
-    stacks, p_ref, c_ref, stream, columns,
-    theirs, ours, summed, in_x, in_y, out_a, out_b, got_x, got_y, block, blocks, cols,
-    ps, pr, as_, ar, bs, br, xs, xr, ys, yr, zs, zr, gs, gr, es, er, local, load,
+    stacks, p_ref, c_ref, m_ref, w_ref, conv_ref, gb_ref, gc_ref, ci_ref, taps_ref,
+    columns, full_m, dgb_ref, dgc_ref, dci_ref,
+    theirs, ours, summed, in_x, in_y, out_a, out_b, got_x, got_y, block, blocks, stream, ext,
+    ps, pr, as_, ar, bs, br, xs, xr, ys, yr, zs, zr, ms, mr, ns, nr, gs, gr, es, er, local, load, hs, hr,
 ):
     sp, z, c, t = place()
     rows, width = p_ref.shape[0] // (2 * stacks), p_ref.shape[1]
@@ -411,6 +409,22 @@
     for k in order:
         swap(k).start()
         read(k).start()
+
+    def behind(k):
+        return lax.rem(z + stacks - k, stacks)
+
+    def merged_out(k):
+        return remote(m_ref, full_m.at[span(z, c), :], ms.at[k], mr.at[k], (2 * other_stack(k) + c, t))
+
+    def merged_on(k):
+        r = full_m.at[span(behind(k), c), :]
+        return remote(r if k else m_ref, r, ns.at[k], nr.at[k], partner)
+
+    for k in range(1, stacks):
+        merged_out(k).start()
+    merged_on(0).start()
+    keep_m = pltpu.make_async_copy(m_ref, full_m.at[span(z, c), :], local.at[0])
+    keep_m.start()
     for i in range(stacks + 2):
         for stage, lag in ((stage_one, 0), (stage_two, 1), (stage_three, 2)):
             if 0 <= i - lag < stacks:
@@ -419,17 +433,18 @@
     for k in range(1, stacks):
         home(k).wait_recv()
         total = total + blocks[k].astype(jnp.float32)
-    cols[...] = total.astype(jnp.bfloat16)
+    stream[:, wide(t)] = total.astype(jnp.bfloat16)
 
     gathers = []
     for i, u in enumerate((td, tx, ty)):
-        gathers.append(remote(cols, stream.at[:, wide(t)], gs.at[i], gr.at[i], (sp, u)))
+        own = stream.at[:, wide(t)]
+        gathers.append(remote(own, own, gs.at[i], gr.at[i], (sp, u)))
         gathers[-1].start()
-    keep = pltpu.make_async_copy(cols, stream.at[:, wide(t)], local.at[0])
-    keep.start()
+    for k in range(1, stacks):
+        merged_out(k).wait_recv()
+        merged_on(k).start()
     for copy in gathers:
         copy.wait()
-    keep.wait()
     share = columns.shape[1]
 
     def slab(device):
@@ -446,6 +461,45 @@
             n += 1
     keep = pltpu.make_async_copy(slab(sp), mine, local.at[1])
     keep.start()
+
+    last = 2 * stacks - 1
+    halo = remote(
+        ext.at[pl.ds(0, 8), :], ext.at[pl.ds(rows, 8), :], hs.at[0], hr.at[0], (jnp.maximum(sp - 1, 0), t)
+    )
+    grad_merged = contract(stream[...], w_ref[...], 1, 1)
+    ext[pl.ds(0, rows), :] = grad_merged * gb_ref[...].astype(jnp.float32)
+
+    @pl.when(sp > 0)
+    def _():
+        halo.start()
+
+    dgb_ref[...] = (grad_merged * conv_ref[...]).astype(jnp.bfloat16)
+
+    @pl.when(sp == last)
+    def _():
+        ext[pl.ds(rows, 8), :] = jnp.zeros((8, quarter), jnp.float32)
+
+    @pl.when(sp < last)
+    def _():
+        halo.wait_recv()
+
+    grad_mixed = (
+        taps_ref[2:3, :] * ext[pl.ds(0, rows), :]
+        + taps_ref[1:2, :] * ext[pl.ds(1, rows), :]
+        + taps_ref[0:1, :] * ext[pl.ds(2, rows), :]
+    )
+    dgc_ref[...] = (grad_mixed * ci_ref[...].astype(jnp.float32)).astype(jnp.bfloat16)
+    dci_ref[...] = (grad_mixed * gc_ref[...].astype(jnp.float32)).astype(jnp.bfloat16)
+
+    @pl.when(sp > 0)
+    def _():
+        halo.wait_send()
+
+    keep_m.wait()
+    for k in range(stacks):
+        if k:
+            merged_out(k).wait_send()
+        merged_on(k).wait()
     for k in order:
         swap(k).wait_send()
         via_x(k).wait_send()
@@ -479,38 +533,38 @@
     conv = taps[2] * mixed + taps[1] * extended[1:-1] + taps[0] * extended[:-2]
     merged = (gate_b.astype(jnp.float32) * conv).astype(bf16)
 
-    ids = lax.all_gather(route_ids, "sp", axis=0, tiled=True)
-    weights = lax.all_gather(route_weights, "sp", axis=0, tiled=True)
-    chosen = jnp.sum(jnp.where(ids == lax.axis_index("sp"), weights, 0.0), axis=1, keepdims=True)
-
-    n = 6 * (stacks - 1)
-    rows_x, all_cot, all_merged = pl.pallas_call(
+    named = jnp.arange(groups, dtype=jnp.int32)[:, None, None] == route_ids.T[None]
+    table = jnp.sum(jnp.where(named, route_weights.T[None], 0.0), axis=1)
+
+    n = 4 * (stacks - 1)
+    rows_x, rows_c, tables = pl.pallas_call(
         functools.partial(gather_kernel, stacks),
         out_shape=(
             jax.ShapeDtypeStruct((tokens, width), bf16),
             jax.ShapeDtypeStruct((tokens, width), bf16),
-            jax.ShapeDtypeStruct((tokens, quarter), bf16),
+            jax.ShapeDtypeStruct((groups, groups, rows), jnp.float32),
         ),
         in_specs=[vmem] * 3,
-        out_specs=(any_space,) * 3,
-        scratch_shapes=[dma((n,))] * 10 + [dma((4 * n,))] * 2 + [dma((3,))] * 3,
+        out_specs=(any_space, any_space, vmem),
+        scratch_shapes=[dma((n,))] * 10 + [dma((4 * n,))] * 2 + [dma((groups - 1,))] * 2 + [dma((3,))] * 3,
         compiler_params=pltpu.CompilerParams(collective_id=0, has_side_effects=True),
-    )(moe_input, cotangent, merged)
-
-    rows_s = (chosen * all_cot.astype(jnp.float32)).astype(bf16)
+    )(moe_input, cotangent, table)
+    chosen = lax.dynamic_index_in_dim(tables, lax.axis_index("sp"), 1, keepdims=False)
+    chosen = chosen.reshape(tokens, 1)
+
     weight_gate, weight_up, weight_down = expert_gate[0], expert_up[0], expert_down[0]
     pre_gate = jnp.dot(rows_x, weight_gate, preferred_element_type=jnp.float32)
     pre_up = jnp.dot(rows_x, weight_up, preferred_element_type=jnp.float32)
     sigma = jax.nn.sigmoid(pre_gate)
     active = pre_gate * sigma
-    hidden = (active * pre_up).astype(bf16)
-    back = contract(rows_s, weight_down, 1, 1)
+    hidden = (chosen * (active * pre_up)).astype(bf16)
+    back = chosen * contract(rows_c, weight_down, 1, 1)
     grad_pre_gate = (back * pre_up * sigma * (1.0 + pre_gate * (1.0 - sigma))).astype(bf16)
     grad_pre_up = (back * active).astype(bf16)
     partial_value = (
         contract(grad_pre_gate, weight_gate, 1, 1) + contract(grad_pre_up, weight_up, 1, 1)
     ).astype(bf16)
-    grad_down = contract(hidden, rows_s, 0, 0)
+    grad_down = contract(hidden, rows_c, 0, 0)
     grad_gate = contract(rows_x, grad_pre_gate, 0, 0)
     grad_up = contract(rows_x, grad_pre_up, 0, 0)
 
@@ -523,29 +577,23 @@
     ]
     scratch += [pltpu.VMEM((stacks, rows, half), bf16)] * 4
     scratch += [pltpu.VMEM((stacks, rows, quarter), bf16)] * 4
-    scratch += [pltpu.VMEM((rows, quarter), bf16)]
-    scratch += [dma((stacks,))] * 12 + [dma((3,))] * 2 + [dma((groups - 1,))] * 2
-    scratch += [dma((2,)), dma((stacks,))]
-    stream_grad, stream_cols = pl.pallas_call(
+    scratch += [pltpu.VMEM((rows, width), bf16), pltpu.VMEM((rows + 8, quarter), jnp.float32)]
+    scratch += [dma((stacks,))] * 16 + [dma((3,))] * 2 + [dma((groups - 1,))] * 2
+    scratch += [dma((2,)), dma((stacks,)), dma((1,)), dma((1,))]
+    token_block = jax.ShapeDtypeStruct((rows, quarter), bf16)
+    stream_cols, all_merged, grad_gate_b, grad_gate_c, grad_conv_in = pl.pallas_call(
         functools.partial(return_kernel, stacks),
         out_shape=(
-            jax.ShapeDtypeStruct((rows, width), bf16),
             jax.ShapeDtypeStruct((tokens, share), bf16),
+            jax.ShapeDtypeStruct((tokens, quarter), bf16),
+            token_block, token_block, token_block,
         ),
-        in_specs=[any_space, vmem],
-        out_specs=(any_space, any_space),
+        in_specs=[any_space] + [vmem] * 8,
+        out_specs=(any_space, any_space, vmem, vmem, vmem),
         scratch_shapes=scratch,
         compiler_params=pltpu.CompilerParams(collective_id=1, has_side_effects=True),
-    )(partial_value, cotangent)
-
-    grad_merged = contract(stream_grad, out_proj, 1, 1)
-    grad_gate_b = (grad_merged * conv).astype(bf16)
-    grad_conv = grad_merged * gate_b.astype(jnp.float32)
-    later_rows = passed_along(grad_conv[:2], "sp", -1)
-    extended_grad = jnp.concatenate([grad_conv, later_rows], axis=0)
-    grad_mixed = taps[2] * grad_conv + taps[1] * extended_grad[1:-1] + taps[0] * extended_grad[2:]
-    grad_gate_c = (grad_mixed * conv_in.astype(jnp.float32)).astype(bf16)
-    grad_conv_in = (grad_mixed * gate_c.astype(jnp.float32)).astype(bf16)
+    )(partial_value, cotangent, merged, out_proj, conv, gate_b, gate_c, conv_in, taps)
+
     grad_proj = contract(all_merged, stream_cols, 0, 0)
     return (
         grad_gate[None], grad_up[None], grad_down[None], grad_proj,

time: 182 us -> 162 us (0.89)
  blocking collectives: 23 us -> 0 us
  matrix products: 28.4 us -> 35.8 us
  starting transfers between devices: 5.68 us -> 3.77 us
  other arithmetic: 5.26 us -> 3.38 us
    all_gather x2 -> x0, blocking collectives: 23 us -> none  [the longest x1 12.9 us: dense_plan(): weights = lax.all_gather(route_weights, 'sp', axis=0, tiled=True)]
    dot_general x8 -> x7, matrix products: 21.9 us -> 27.5 us  [contract(): lax.dot_general(left, right, (((left_dim,), (right_dim,)), ((), ())), pre...]
    ppermute x2 -> x1, starting transfers between devices: 5.68 us -> 3.77 us  [passed_along(): return lax.ppermute(block, axis, route)]
  transfers between devices with their start and end apart: 2 -> 1, of which waited for: 1 -> 0; matrix products, arithmetic and copies ran while one was open for 1% -> 22% of each run, Pallas kernels for 0% -> 31%
where the time goes in v2:
time: 162 us
  Pallas kernels  115 us (71%)
  matrix products  35.8 us (22%)
  starting transfers between devices  3.77 us (2%)
  other arithmetic  3.38 us (2%)
  local copies, waits for them, and re-layouts  3.04 us (2%)
    pallas_call x1, Pallas kernels, dense_plan(): pl.pallas_call(functools.partial(return_kernel, stacks), out_shape=(jax.S...  65.3 us
    pallas_call x1, Pallas kernels, dense_plan(): pl.pallas_call(functools.partial(gather_kernel, stacks), out_shape=(jax.S...  49.9 us
    dot_general x7, matrix products, contract(): lax.dot_general(left, right, (((left_dim,), (right_dim,)), ((), ())), pre...  27.5 us
    dot_general x1, matrix products, dense_plan(): pre_gate = jnp.dot(rows_x, weight_gate, preferred_element_type=jnp.float32)  5.55 us
    ppermute x1, starting transfers between devices, passed_along(): return lax.ppermute(block, axis, route)  3.77 us
  transfers between devices with their start and end apart: 1, of which 0 were waited for; matrix products, arithmetic and copies ran while one was open for 22% of the time, Pallas kernels for 31%

profile of v2, /device:TPU:19, one launch (start us, length us, event | category | flops | bytes accessed | tf_op | source)
XLA Modules:
  0.0 162.0 jit_solution(11079678163837389637)
XLA Ops:
  0.6 0.0 copy-start
  0.6 1.1 convert_multiply_fusion
  1.8 3.8 %collective-permute-start = (f32[2,512]{1,0:T(2,128)S(1)}, f32[2,512]{1,0:T(2,128)S(1)}, u32[]{:S(2)}, u32[]{:S(2)}) collective-permute-start(f32[2,512]{1,0:T(2,128)S(1)} %slice.24), channel_id=1, source_target_pairs={{0,4},{4,8},{8,12},{12,16},{16,20},{20,24},{24,28},{1,5},{5,9},{9,... | collective-permute-start | bytes 12296 | tf_op jit(solution)/shard_map/ppermute | solution.py:15
  5.6 1.3 select_reduce_fusion.w_ref
  6.9 49.9 %shard_map.171 = (bf16[1408,2048]{1,0:T(8,128)(2,1)}, bf16[1408,2048]{1,0:T(8,128)(2,1)}, f32[8,8,176]{2,1,0:T(8,128)}) custom-call(bf16[176,2048]{1,0:T(8,128)(2,1)} %x_ref.1, bf16[176,2048]{1,0:T(8,128)(2,1)} %c_ref.1, f32[8,176]{1,0:T(8,128)} %select_reduce_fusion.w_ref), custom_call_target="tpu_custom_call" | custom-call | tf_op jit(solution)/shard_map/pallas_call | solution.py:540
  56.8 0.0 copy-done
  56.8 0.0 copy-start.1
  56.8 0.0 copy-start.7
  56.8 5.5 %fusion.3 = f32[1408,256]{1,0:T(8,128)} fusion(bf16[1408,2048]{1,0:T(8,128)(2,1)} %get-tuple-element.15, bf16[1,2048,256]{2,1,0:T(8,128)(2,1)S(1)} %copy-done), kind=kOutput, calls=%fused_computation.12 | convolution fusion | flops 1476395008 | bytes 8257536 | tf_op jit(solution)/shard_map/dot_general | solution.py:556
  62.4 0.0 copy-done.1
  62.4 0.0 copy-done.7
  62.4 2.8 %fusion.6 = f32[1408,256]{1,0:T(8,128)} fusion(bf16[1408,2048]{1,0:T(8,128)(2,1)S(1)} %copy-done.7, bf16[1,2048,256]{2,1,0:T(8,128)(2,1)S(1)} %copy-done.1), kind=kOutput, calls=%fused_computation.15 | convolution fusion | flops 1476395008 | bytes 8257536 | tf_op jit(solution)/shard_map/dot_general | solution.py:557
  65.2 0.9 dynamic-slice_reduce_fusion
  66.1 0.1 mul.73
  66.1 0.0 copy-start.8
  66.2 0.0 copy-start.9
  66.2 0.0 copy-start.10
  66.2 0.0 slice-start
  66.2 6.9 %convolution_bitcast_fusion = f32[1,256,2048]{2,1,0:T(8,128)} fusion(bf16[1408,2048]{1,0:T(8,128)(2,1)} %get-tuple-element.17, f32[1408,256]{1,0:T(8,128)} %fusion.6, f32[1408]{0:T(1024)S(1)} %mul.73, f32[1408,256]{1,0:T(8,128)} %fusion.3), kind=kOutput, calls=%fused_computation.2 | convolution fusion | flops 1478918144 | bytes 10753536 | tf_op jit(solution)/shard_map/dot_general | solution.py:26
  73.1 0.0 copy-done.8
  73.1 0.0 copy-done.9
  73.1 0.0 copy-done.10
  73.1 0.0 slice-start.1
  73.1 5.1 %multiply_convert_fusion.1 = (bf16[1408,256]{1,0:T(8,128)(2,1)S(1)}, bf16[1408,256]{1,0:T(8,128)(2,1)S(1)}) fusion(f32[1408,256]{1,0:T(8,128)S(1)} %copy-done.9, f32[1408,256]{1,0:T(8,128)S(1)} %copy-done.10, bf16[1408,2048]{1,0:T(8,128)(2,1)} %get-tuple-element.17, bf16[1,256,2048]{2,1,0:T(8,128)(2,1)S(1)} %copy-done.8, f32[1408]{0:T(1024)S(1)} %mul.73), kind=kOutput, calls=%fused_computation.6 | convolution fusion | flops 1481441280 | bytes 11146752 | tf_op jit(solution)/shard_map/dot_general | solution.py:26
  78.2 0.0 slice-done
  78.2 0.0 slice-done.1
  78.2 3.2 %convolution_bitcast_fusion.2 = f32[1,2048,256]{2,1,0:T(8,128)} fusion(bf16[1408,2048]{1,0:T(8,128)(2,1)S(1)} %bitcast.44, bf16[1408,256]{1,0:T(8,128)(2,1)S(1)} %get-tuple-element.26), kind=kOutput, calls=%fused_computation.4 | convolution fusion | flops 1476395008 | bytes 8585216 | tf_op jit(solution)/shard_map/dot_general | solution.py:26
  81.4 1.7 %fusion.1 = f32[1408,2048]{1,0:T(8,128)S(1)} fusion(bf16[1408,256]{1,0:T(8,128)(2,1)S(1)} %get-tuple-element.26, bf16[1,2048,256]{2,1,0:T(8,128)(2,1)S(1)} %copy-done), kind=kOutput, calls=%fused_computation.10 | convolution fusion | flops 1476395008 | bytes 13303808 | tf_op jit(solution)/shard_map/dot_general | solution.py:26
  83.1 3.4 %convolution_bitcast_fusion.1 = f32[1,2048,256]{2,1,0:T(8,128)} fusion(bf16[1408,2048]{1,0:T(8,128)(2,1)S(1)} %bitcast.44, bf16[1408,256]{1,0:T(8,128)(2,1)S(1)} %get-tuple-element.25), kind=kOutput, calls=%fused_computation.3 | convolution fusion | flops 1476395008 | bytes 8585216 | tf_op jit(solution)/shard_map/dot_general | solution.py:26
  86.5 0.0 copy-start.6
  86.5 0.0 copy-start.2
  86.5 4.2 %add_convert_fusion.p_ref = bf16[1408,2048]{1,0:T(8,128)(2,1)} fusion(f32[1408,2048]{1,0:T(8,128)S(1)} %fusion.1, bf16[1408,256]{1,0:T(8,128)(2,1)S(1)} %get-tuple-element.25, bf16[1,2048,256]{2,1,0:T(8,128)(2,1)S(1)} %copy-done.1), kind=kOutput, calls=%fused_computation | convolution fusion | flops 1482162176 | bytes 19070976 | tf_op jit(solution)/shard_map/dot_general | solution.py:26
  90.7 0.0 copy-done.6
  90.7 0.0 collective-permute-done
  90.7 0.0 copy-done.2
  90.7 0.9 multiply_convert_fusion.4
  91.7 65.3 %shard_map.172 = (bf16[1408,256]{1,0:T(8,128)(2,1)}, bf16[1408,512]{1,0:T(8,128)(2,1)}, bf16[176,512]{1,0:T(8,128)(2,1)}, bf16[176,512]{1,0:T(8,128)(2,1)}, bf16[176,512]{1,0:T(8,128)(2,1)}) custom-call(bf16[1408,2048]{1,0:T(8,128)(2,1)} %add_convert_fusion.p_ref, bf16[176,2048]{1,0:T(8,128)(2,1)} %c_ref.1, bf16[176,512]{1,0:T(8,128)(2,1)} %get-tuple-element.23.m_ref, ...), custom_call_target="tpu_custom_call" | custom-call | tf_op jit(solution)/shard_map/pallas_call | solution.py:584
  157.0 0.0 copy-start.5
  157.0 0.0 copy-start.4
  157.0 0.0 copy-start.3
  157.0 3.0 %fusion.19 = f32[512,256]{1,0:T(8,128)} fusion(bf16[1408,512]{1,0:T(8,128)(2,1)} %get-tuple-element.18, bf16[1408,256]{1,0:T(8,128)(2,1)} %get-tuple-element.19), kind=kOutput, calls=%fused_computation.34 | convolution fusion | flops 369098752 | bytes 2686976 | tf_op jit(solution)/shard_map/dot_general | solution.py:26
  160.0 0.0 copy-done.5
  160.0 0.7 copy.22
  160.7 0.0 copy-done.4
  160.7 0.7 copy.23
  161.3 0.0 copy-done.3
  161.3 0.7 copy.24
  (3 shorter events, 0.0 us)
Async XLA Ops:
  0.6 56.2 %copy-start = (bf16[1,2048,256]{2,1,0:T(8,128)(2,1)S(1)}, bf16[1,2048,256]{2,1,0:T(8,128)(2,1)}, u32[]{:S(2)}) copy-start(bf16[1,2048,256]{2,1,0:T(8,128)(2,1)} %param.16) | copy-start | bytes 3145732
  1.8 88.9 %collective-permute-start = (f32[2,512]{1,0:T(2,128)S(1)}, f32[2,512]{1,0:T(2,128)S(1)}, u32[]{:S(2)}, u32[]{:S(2)}) collective-permute-start(f32[2,512]{1,0:T(2,128)S(1)} %slice.24), channel_id=1, source_target_pairs={{0,4},{4,8},{8,12},{12,16},{16,20},{20,24},{24,28},{1,5},{5,9},{9,... | collective-permute-start | bytes 12296 | tf_op jit(solution)/shard_map/ppermute | solution.py:15
  56.8 5.6 %copy-start.1 = (bf16[1,2048,256]{2,1,0:T(8,128)(2,1)S(1)}, bf16[1,2048,256]{2,1,0:T(8,128)(2,1)}, u32[]{:S(2)}) copy-start(bf16[1,2048,256]{2,1,0:T(8,128)(2,1)} %param.17) | copy-start | bytes 3145732
  56.8 5.6 %copy-start.7 = (bf16[1408,2048]{1,0:T(8,128)(2,1)S(1)}, bf16[1408,2048]{1,0:T(8,128)(2,1)}, u32[]{:S(2)}) copy-start(bf16[1408,2048]{1,0:T(8,128)(2,1)} %get-tuple-element.15) | copy-start | bytes 17301508
  66.1 7.0 %copy-start.8 = (bf16[1,256,2048]{2,1,0:T(8,128)(2,1)S(1)}, bf16[1,256,2048]{2,1,0:T(8,128)(2,1)}, u32[]{:S(2)}) copy-start(bf16[1,256,2048]{2,1,0:T(8,128)(2,1)} %param.18) | copy-start | bytes 3145732
  66.2 6.9 %copy-start.9 = (f32[1408,256]{1,0:T(8,128)S(1)}, f32[1408,256]{1,0:T(8,128)}, u32[]{:S(2)}) copy-start(f32[1408,256]{1,0:T(8,128)} %fusion.3) | copy-start | bytes 4325380
  66.2 6.9 %copy-start.10 = (f32[1408,256]{1,0:T(8,128)S(1)}, f32[1408,256]{1,0:T(8,128)}, u32[]{:S(2)}) copy-start(f32[1408,256]{1,0:T(8,128)} %fusion.6) | copy-start | bytes 4325380
  66.2 12.0 %slice-start = ((s8[5767168]{0:T(1024)(128)(4,1)}), s8[4194304]{0:T(1024)(128)(4,1)S(1)}, s32[]{:S(2)}) async-start(s8[5767168]{0:T(1024)(128)(4,1)} %bitcast.43), calls=%async_computation | async-start | bytes 8388608
  73.1 5.1 %slice-start.1 = ((s8[5767168]{0:T(1024)(128)(4,1)}), s8[1572864]{0:T(1024)(128)(4,1)S(1)}, s32[]{:S(2)}) async-start(s8[5767168]{0:T(1024)(128)(4,1)} %bitcast.43), calls=%async_computation.1 | async-start | bytes 3145728
  86.5 4.2 %copy-start.6 = (f32[3,512]{1,0:T(4,128)S(1)}, f32[3,512]{1,0:T(4,128)}, u32[]{:S(2)}) copy-start(f32[3,512]{1,0:T(4,128)} %taps_ref.1) | copy-start | bytes 18436
  86.5 4.2 %copy-start.2 = (bf16[176,512]{1,0:T(8,128)(2,1)S(1)}, bf16[176,512]{1,0:T(8,128)(2,1)}, u32[]{:S(2)}) copy-start(bf16[176,512]{1,0:T(8,128)(2,1)} %gb_ref.1) | copy-start | bytes 540676
  157.0 3.0 %copy-start.5 = (bf16[176,512]{1,0:T(8,128)(2,1)S(1)}, bf16[176,512]{1,0:T(8,128)(2,1)}, u32[]{:S(2)}) copy-start(bf16[176,512]{1,0:T(8,128)(2,1)} %get-tuple-element.41) | copy-start | bytes 540676
  157.0 3.7 %copy-start.4 = (bf16[176,512]{1,0:T(8,128)(2,1)S(1)}, bf16[176,512]{1,0:T(8,128)(2,1)}, u32[]{:S(2)}) copy-start(bf16[176,512]{1,0:T(8,128)(2,1)} %get-tuple-element.42) | copy-start | bytes 540676
  157.0 4.4 %copy-start.3 = (bf16[176,512]{1,0:T(8,128)(2,1)S(1)}, bf16[176,512]{1,0:T(8,128)(2,1)}, u32[]{:S(2)}) copy-start(bf16[176,512]{1,0:T(8,128)(2,1)} %get-tuple-element.43) | copy-start | bytes 540676
